TPU v7x, 256 devices: a whole 4x4x8 slice. The times are simulated.
256 devices in a mesh: kv: 16 (over y, x), tp: 16 (over z, core).
Axes of the slice: x: 4, y: 4, z: 8, core: 2. Of those that a mesh axis runs over, the one named last changes fastest.
Arguments:
- tokens: bfloat16 [128, 4096], P(None, ('kv', 'tp')), may hold values from -41 to 41
- lengths: int32 [128], P('kv'), may hold values from 1 to 8192, 262144 in all
- retention_state: float32 [128, 16, 128, 256], P('kv', 'tp'), may hold values from -4 to 4
- mixer_gain: float32 [4096], P('kv'), may hold values from 0.1 to 1.9
- query_weight: bfloat16 [4096, 2048], P('kv', 'tp'), may hold values from -0.09375 to 0.09375
- key_weight: bfloat16 [4096, 2048], P('kv', 'tp'), may hold values from -0.09375 to 0.09375
- value_weight: bfloat16 [4096, 4096], P('kv', 'tp'), may hold values from -0.09375 to 0.09375
- gate_weight: bfloat16 [4096, 4096], P('kv', 'tp'), may hold values from -0.09375 to 0.09375
- output_weight: bfloat16 [4096, 4096], P('tp', 'kv'), may hold values from -0.125 to 0.125
- channel_gain: float32 [4096], P('kv'), may hold values from 0.1 to 1.9
- ffn_gate: bfloat16 [4096, 11264], P('kv', 'tp'), may hold values from -0.09375 to 0.09375
- ffn_up: bfloat16 [4096, 11264], P('kv', 'tp'), may hold values from -0.09375 to 0.09375
- ffn_down: bfloat16 [11264, 4096], P('tp', 'kv'), may hold values from -0.078125 to 0.078125
Outputs:
- layer_output: bfloat16 [128, 4096], P(None, ('kv', 'tp'))
- new_state: float32 [128, 16, 128, 256], P('kv', 'tp')
All inputs are finite; a program needn't handle non-finite values. No bound on the sum of `lengths` on one device may be relied on, other than what follows from the above.
Results may differ from a plain program's by a relative error of at most 0.022.
Values may be sent and summed in bfloat16 or wider, within the bound.
No kernel may reach another device: no remote copies, remote signals or barrier semaphores. Data moves between devices by JAX's collectives and lax.ppermute only.
A program may use at most 64 MiB of HBM per device.

v0:
```python
import jax
import jax.numpy as jnp
from jax import lax
from jax.sharding import PartitionSpec as P

D = 4096
HEADS = 16
QK = 128


def in_blocks(value, dim, devices):
    lengths = value.shape
    blocks = value.reshape(*lengths[:dim], devices, lengths[dim] // devices, *lengths[dim + 1 :])
    return jnp.moveaxis(blocks, dim, 0)


def sent_and_summed(value, axis, dim):
    blocks = in_blocks(value, dim, lax.axis_size(axis))
    arrived = lax.all_to_all(blocks, axis, split_axis=0, concat_axis=0, tiled=True)
    return arrived.astype(jnp.float32).sum(axis=0)


def in_one_piece(arrays, axis, dim, along):
    columns = [a.reshape(*a.shape[:along], -1) for a in arrays]
    both = jnp.concatenate(columns, axis=along)
    result, at, finished = (sent_and_summed(both, axis, dim), 0, [])
    for a, column in zip(arrays, columns):
        piece = result[..., at : at + column.shape[along]]
        finished.append(piece.reshape(*piece.shape[:along], *a.shape[along:]))
        at += column.shape[along]
    return tuple(finished)


def copy_for_each(value, axis):
    devices = lax.axis_size(axis)
    return lax.all_to_all(
        jnp.broadcast_to(value[None], (devices, *value.shape)), axis, 0, 0, tiled=True
    )


def joined_along(blocks, dim):
    blocks = jnp.moveaxis(blocks, 0, dim)
    lengths = blocks.shape
    return blocks.reshape(*lengths[:dim], lengths[dim] * lengths[dim + 1], *lengths[dim + 2 :])


def gather_directly(value, axis, dim):
    blocks = copy_for_each(value, axis)
    return joined_along(blocks, dim)


def rotate_heads(vectors, positions):
    half_dim = vectors.shape[-1] // 2
    frequency = 10000.0 ** (-jnp.arange(half_dim, dtype=jnp.float32) / half_dim)
    angles = positions.astype(jnp.float32)[:, None, None] * frequency
    cosine = jnp.cos(angles)
    sine_part = jnp.sin(angles)
    first_half = vectors[..., :half_dim]
    second = vectors[..., half_dim:]
    return jnp.concatenate(
        [first_half * cosine - second * sine_part, first_half * sine_part + second * cosine],
        axis=-1,
    )


def gathered_rows(columns):
    return lax.all_gather(columns, "tp", axis=1, tiled=True)


def owned_sums(partial_value, squares):
    raw_sums, totals = in_one_piece(
        (partial_value.astype(jnp.bfloat16), squares.astype(jnp.bfloat16)), "kv", 0, 1
    )
    summed = raw_sums * lax.rsqrt(totals / D + 1e-06)[:, None]
    return summed


def on_device(
    tokens,
    lengths,
    retention_state,
    mixer_gain,
    query_weight,
    key_weight,
    value_weight,
    gate_weight,
    output_weight,
    channel_gain,
    ffn_gate,
    ffn_up,
    ffn_down,
):
    feature_block = gathered_rows(tokens).astype(jnp.float32)
    squares = jnp.sum(feature_block * feature_block, axis=1)
    normed = (feature_block * mixer_gain).astype(jnp.bfloat16)
    partial_value = jnp.concatenate(
        [
            jnp.dot(normed, query_weight, preferred_element_type=jnp.float32),
            jnp.dot(normed, key_weight, preferred_element_type=jnp.float32),
            jnp.dot(normed, value_weight, preferred_element_type=jnp.float32),
            jnp.dot(normed, gate_weight, preferred_element_type=jnp.float32),
        ],
        axis=1,
    )
    owned_rows = owned_sums(partial_value, squares)
    local_heads = query_weight.shape[1] // QK
    q_width = query_weight.shape[1]
    v_width = value_weight.shape[1]
    head_width = v_width // local_heads
    seq_rows = owned_rows.shape[0]
    query_rows = rotate_heads(
        owned_rows[:, :q_width].reshape(seq_rows, local_heads, QK), lengths
    ).astype(jnp.bfloat16)
    key_rows = (
        rotate_heads(
            owned_rows[:, q_width : 2 * q_width].reshape(seq_rows, local_heads, QK), lengths
        )
        * QK ** (-0.5)
    ).astype(jnp.bfloat16)
    value_rows = (
        owned_rows[:, 2 * q_width : 2 * q_width + v_width]
        .astype(jnp.bfloat16)
        .reshape(seq_rows, local_heads, head_width)
    )
    gate_rows = owned_rows[:, 2 * q_width + v_width :]
    head_ids = (lax.axis_index("tp") * local_heads + jnp.arange(local_heads)).astype(jnp.float32)
    decay_rate = 1.0 - 2.0 ** (-5.0 - 10.0 * head_ids / (HEADS - 1))
    new_state = (
        decay_rate[None, :, None, None] * retention_state
        + key_rows.astype(jnp.float32)[..., :, None] * value_rows.astype(jnp.float32)[..., None, :]
    )
    retained = jnp.einsum(
        "bhk,bhkv->bhv", query_rows.astype(jnp.float32), new_state, precision=lax.Precision.HIGHEST
    )
    normalized = retained * lax.rsqrt(jnp.mean(retained * retained, axis=-1) + 1e-06)[..., None]
    merged = (normalized.reshape(seq_rows, v_width) * jax.nn.silu(gate_rows)).astype(jnp.bfloat16)
    mixed_part = jnp.dot(
        gather_directly(merged, "kv", 0), output_weight, preferred_element_type=jnp.float32
    )
    mixed_cols = sent_and_summed(mixed_part.astype(jnp.bfloat16), "tp", 1)
    residual = (tokens.astype(jnp.float32) + mixed_cols).astype(jnp.bfloat16)
    block_two = gathered_rows(residual).astype(jnp.float32)
    squares_two = jnp.sum(block_two * block_two, axis=1)
    normed_two = (block_two * channel_gain).astype(jnp.bfloat16)
    partial_two = jnp.concatenate(
        [
            jnp.dot(normed_two, ffn_gate, preferred_element_type=jnp.float32),
            jnp.dot(normed_two, ffn_up, preferred_element_type=jnp.float32),
        ],
        axis=1,
    )
    hidden_units = ffn_gate.shape[1]
    summed = owned_sums(partial_two, squares_two)
    hidden = (jax.nn.silu(summed[:, :hidden_units]) * summed[:, hidden_units:]).astype(jnp.bfloat16)
    down_part = jnp.dot(
        gather_directly(hidden, "kv", 0), ffn_down, preferred_element_type=jnp.float32
    )
    down_sums = sent_and_summed(down_part.astype(jnp.bfloat16), "tp", 1)
    layer_output = (residual.astype(jnp.float32) + down_sums).astype(jnp.bfloat16)
    return (layer_output, new_state)


def solution(mesh):
    in_specs = (
        P(None, ("kv", "tp")),
        P("kv"),
        P("kv", "tp", None, None),
        P("kv"),
        P("kv", "tp"),
        P("kv", "tp"),
        P("kv", "tp"),
        P("kv", "tp"),
        P("tp", "kv"),
        P("kv"),
        P("kv", "tp"),
        P("kv", "tp"),
        P("tp", "kv"),
    )
    out_specs = (P(None, ("kv", "tp")), P("kv", "tp", None, None))
    return jax.shard_map(
        on_device, mesh=mesh, in_specs=in_specs, out_specs=out_specs, check_vma=False
    )
```

profile of v0, /device:TPU:1, one launch (start us, length us, event | category | flops | bytes accessed | tf_op | source)
XLA Modules:
  0.0 126.4 jit_solution(4354620266394448964)
XLA Ops:
  0.7 21.8 %all_gather.6 = bf16[128,256]{0,1:T(8,128)(2,1)S(1)} all-gather(bf16[128,16]{0,1:T(8,128)(2,1)} %param.13), channel_id=1, replica_groups=mesh['kv'=16,'tp'=16] {'tp'}, dimensions={1}, use_global_device_ids=true | all-gather | bytes 69632 | tf_op jit(solution)/shard_map/all_gather | solution.py:67
  22.6 0.2 convert_element_type.141
  22.8 1.8 %fusion.5 = bf16[16,8,769]{2,1,0:T(8,128)(2,1)} fusion(bf16[256,128]{1,0:T(8,128)(2,1)} %param.17, bf16[128,256]{0,1:T(8,128)(2,1)S(1)} %all_gather.6, f32[256]{0:T(256)} %param.16), kind=kOutput, calls=%fused_computation.13 | convolution fusion | flops 8503295 | bytes 164864 | tf_op jit(solution)/shard_map/dot_general | solution.py:98
  24.6 1.8 %fusion.7 = bf16[16,8,769]{2,1,0:T(8,128)(2,1)} fusion(bf16[16,8,769]{2,1,0:T(8,128)(2,1)} %fusion.5, bf16[256,128]{1,0:T(8,128)(2,1)} %param.18, bf16[128,256]{0,1:T(8,128)(2,1)S(1)} %all_gather.6, f32[256]{0:T(256)} %param.16), kind=kOutput, calls=%fused_computation.15 | convolution fusion | flops 8503296 | bytes 164864 | tf_op jit(solution)/shard_map/dot_general | solution.py:99
  26.3 1.8 %fusion.1 = bf16[16,8,769]{2,1,0:T(8,128)(2,1)} fusion(bf16[16,8,769]{2,1,0:T(8,128)(2,1)} %fusion.7, bf16[256,256]{1,0:T(8,128)(2,1)} %param.19, bf16[128,256]{0,1:T(8,128)(2,1)S(1)} %all_gather.6, f32[256]{0:T(256)} %param.16), kind=kOutput, calls=%fused_computation.7 | convolution fusion | flops 16908288 | bytes 263168 | tf_op jit(solution)/shard_map/dot_general | solution.py:100
  28.1 1.8 %fusion.3 = bf16[16,8,769]{2,1,0:T(8,128)(2,1)} fusion(bf16[16,8,769]{2,1,0:T(8,128)(2,1)} %fusion.1, bf16[256,256]{1,0:T(8,128)(2,1)} %param.20, bf16[128,256]{0,1:T(8,128)(2,1)S(1)} %all_gather.6, f32[256]{0:T(256)} %param.16), kind=kOutput, calls=%fused_computation.9 | convolution fusion | flops 16908288 | bytes 263168 | tf_op jit(solution)/shard_map/dot_general | solution.py:101
  30.0 0.6 constant_dynamic-update-slice_fusion
  30.6 6.8 %all-to-all-start = ((bf16[16,8,769]{2,1,0:T(8,128)(2,1)}), bf16[16,8,769]{2,1,0:T(8,128)(2,1)S(1)}, u32[]{:S(2)}, u32[]{:S(2)}) async-start(bf16[16,8,769]{2,1,0:T(8,128)(2,1)} %constant_dynamic-update-slice_fusion), calls=%async_computation | async-start | bytes 458752 | tf_op jit(solution)/shard_map/all_to_all | solution.py:19
  37.4 0.6 copy-done.8
  38.1 7.3 %all-to-all-done = bf16[16,8,769]{2,1,0:T(8,128)(2,1)S(1)} async-done(((bf16[16,8,769]{2,1,0:T(8,128)(2,1)}), bf16[16,8,769]{2,1,0:T(8,128)(2,1)S(1)}, u32[]{:S(2)}, u32[]{:S(2)}) %all-to-all-start) | async-done | bytes 196896 | tf_op jit(solution)/shard_map/all_to_all | solution.py:19
  45.4 0.1 fusion.44
  45.9 0.2 multiply_add_fusion
  46.1 0.5 fusion.8
  46.8 9.2 %all_to_all.30 = bf16[16,8,256]{2,1,0:T(8,128)(2,1)S(1)} all-to-all(bf16[16,8,256]{2,1,0:T(8,128)(2,1)S(1)} %broadcast_in_dim.4), channel_id=1, replica_groups=mesh['kv'=16,'tp'=16] {'kv'}, dimensions={0} | all-to-all | bytes 131072 | tf_op jit(solution)/shard_map/all_to_all | solution.py:36
  56.0 0.2 convolution_convert_fusion.3
  56.1 0.1 copy.37
  56.2 13.9 %all_to_all.31 = bf16[16,128,16]{1,2,0:T(8,128)(2,1)S(1)} all-to-all(bf16[16,128,16]{1,2,0:T(8,128)(2,1)S(1)} %bitcast.66), channel_id=1, replica_groups=mesh['kv'=16,'tp'=16] {'tp'}, dimensions={0} | all-to-all | bytes 131072 | tf_op jit(solution)/shard_map/all_to_all | solution.py:19
  70.2 0.7 copy-done.6
  70.9 14.9 %all_gather.7 = bf16[128,256]{0,1:T(8,128)(2,1)S(1)} all-gather(bf16[128,16]{0,1:T(8,128)(2,1)S(1)} %add_convert_fusion.1), channel_id=1, replica_groups=mesh['kv'=16,'tp'=16] {'tp'}, dimensions={1}, use_global_device_ids=true | all-gather | bytes 69632 | tf_op jit(solution)/shard_map/all_gather | solution.py:67
  85.8 0.2 convert_element_type.142
  86.0 0.4 copy-done.7
  86.5 0.3 convolution_convert_fusion.1
  86.8 0.1 copy.38
  86.9 0.5 copy-done.3
  87.4 0.3 convolution_convert_fusion
  87.8 0.1 copy.39
  87.9 0.2 concatenate.65
  88.1 12.3 %all_to_all.32 = bf16[16,8,1409]{2,1,0:T(8,128)(2,1)S(1)} all-to-all(bf16[16,8,1409]{2,1,0:T(8,128)(2,1)S(1)} %concatenate.65), channel_id=1, replica_groups=mesh['kv'=16,'tp'=16] {'kv'}, dimensions={0} | all-to-all | bytes 721408 | tf_op jit(solution)/shard_map/all_to_all | solution.py:19
  100.8 10.4 %all_to_all.33 = bf16[16,8,704]{2,1,0:T(8,128)(2,1)S(1)} all-to-all(bf16[16,8,704]{2,1,0:T(8,128)(2,1)S(1)} %broadcast_in_dim.5), channel_id=1, replica_groups=mesh['kv'=16,'tp'=16] {'kv'}, dimensions={0} | all-to-all | bytes 360448 | tf_op jit(solution)/shard_map/all_to_all | solution.py:36
  111.1 0.2 convolution_convert_fusion.2
  111.5 14.3 %all_to_all.34 = bf16[16,128,16]{1,2,0:T(8,128)(2,1)S(1)} all-to-all(bf16[16,128,16]{1,2,0:T(8,128)(2,1)S(1)} %bitcast.67), channel_id=1, replica_groups=mesh['kv'=16,'tp'=16] {'tp'}, dimensions={0} | all-to-all | bytes 131072 | tf_op jit(solution)/shard_map/all_to_all | solution.py:19
  125.8 0.6 add_convert_fusion
  (38 shorter events, 1.2 us)
Async XLA Ops:
  0.6 85.4 %copy-start = (bf16[256,704]{0,1:T(8,128)(2,1)S(1)}, bf16[256,704]{0,1:T(8,128)(2,1)}, u32[]{:S(2)}) copy-start(bf16[256,704]{0,1:T(8,128)(2,1)} %param.23) | copy-start | bytes 1081348
  0.6 45.2 %copy-start.2 = (f32[8,1,128,256]{3,2,1,0:T(8,128)S(1)}, f32[8,1,128,256]{3,2,1,0:T(8,128)}, u32[]{:S(2)}) copy-start(f32[8,1,128,256]{3,2,1,0:T(8,128)} %param.15) | copy-start | bytes 3145732
  30.6 14.7 %all-to-all-start = ((bf16[16,8,769]{2,1,0:T(8,128)(2,1)}), bf16[16,8,769]{2,1,0:T(8,128)(2,1)S(1)}, u32[]{:S(2)}, u32[]{:S(2)}) async-start(bf16[16,8,769]{2,1,0:T(8,128)(2,1)} %constant_dynamic-update-slice_fusion), calls=%async_computation | async-start | bytes 458752 | tf_op jit(solution)/shard_map/all_to_all | solution.py:19
  37.4 0.7 copy-start.8
  46.1 40.7 %copy-start.1 = (f32[8,1,128,256]{3,2,1,0:T(8,128)}, f32[8,1,128,256]{3,2,1,0:T(8,128)S(1)}, u32[]{:S(2)}) copy-start(f32[8,1,128,256]{3,2,1,0:T(8,128)S(1)} %multiply_add_fusion) | copy-start | bytes 3145732
  46.6 9.4 %copy-start.5 = (bf16[256,256]{1,0:T(8,128)(2,1)S(1)}, bf16[256,256]{1,0:T(8,128)(2,1)}, u32[]{:S(2)}) copy-start(bf16[256,256]{1,0:T(8,128)(2,1)} %param.21) | copy-start | bytes 393220
  70.2 0.7 copy-start.6
  85.8 0.7 copy-start.7
  86.5 1.0 copy-start.3
  100.6 10.6 %copy-start.4 = (bf16[704,256]{1,0:T(8,128)(2,1)S(1)}, bf16[704,256]{1,0:T(8,128)(2,1)}, u32[]{:S(2)}) copy-start(bf16[704,256]{1,0:T(8,128)(2,1)} %param.25) | copy-start | bytes 1081348
where the time goes:
time: 127 us; the launch traced here: 126 us
  blocking collectives  96.8 us (76%)
  matrix products  8.66 us (7%)
  waiting for transfers between devices  7.25 us (6%)
  starting transfers between devices  6.75 us (5%)
  local copies, waits for them, and re-layouts  4.08 us (3%)
  other arithmetic  1.99 us (2%)
    all_to_all x3, blocking collectives, sent_and_summed(): lax.all_to_all(blocks, axis, split_axis=0, concat_axis=0, tiled=True)  40.5 us
    all_gather x2, blocking collectives, gathered_rows(): return lax.all_gather(columns, 'tp', axis=1, tiled=True)  36.7 us
    all_to_all x2, blocking collectives, copy_for_each(): lax.all_to_all(jnp.broadcast_to(value[None], (devices, *value.shape)), ax...  19.6 us
    all_to_all x1, waiting for transfers between devices, sent_and_summed(): lax.all_to_all(blocks, axis, split_axis=0, concat_axis=0, tiled=True)  7.25 us
    all_to_all x1, starting transfers between devices, sent_and_summed(): lax.all_to_all(blocks, axis, split_axis=0, concat_axis=0, tiled=True)  6.75 us
  transfers between devices with their start and end apart: 1, of which 1 were waited for; matrix products, arithmetic and copies ran while one was open for 0% of the time, Pallas kernels for 0%

commit v1 on v0

--- a/solution.py
+++ b/solution.py
@@ -64,7 +64,9 @@
 
 
 def gathered_rows(columns):
-    return lax.all_gather(columns, "tp", axis=1, tiled=True)
+    return jnp.concatenate(
+        lax.all_to_all(jnp.stack([columns] * lax.axis_size("tp")), "tp", 0, 0), axis=1
+    )
 
 
 def owned_sums(partial_value, squares):

time: 127 us -> 114 us (0.90)
  blocking collectives: 96.8 us -> 85.4 us
  matrix products: 8.66 us -> 4.5 us
  local copies, waits for them, and re-layouts: 4.08 us -> 6.77 us
    all_gather x2 -> x0, blocking collectives: 36.7 us -> none  [gathered_rows(): return lax.all_gather(columns, 'tp', axis=1, tiled=True)]
    all_to_all x0 -> x2, blocking collectives: none -> 27.9 us  [gathered_rows(): lax.all_to_all(jnp.stack([columns] * lax.axis_size('tp')), 'tp', 0, 0)]
    all_to_all x3, blocking collectives: 40.5 us -> 37.9 us  [sent_and_summed(): lax.all_to_all(blocks, axis, split_axis=0, concat_axis=0, tiled=True)]
    convert_element_type x0 -> x4, local copies, waits for them, and re-layouts: none -> 1.85 us  [the longest x2 0.92 us: on_device(): feature_block = gathered_rows(tokens).astype(jnp.float32)]
    unnamed x18 -> x28, local copies, waits for them, and re-layouts: 2.27 us -> 2.66 us
where the time goes in v1:
time: 114 us
  blocking collectives  85.4 us (75%)
  waiting for transfers between devices  7.3 us (6%)
  local copies, waits for them, and re-layouts  6.77 us (6%)
  starting transfers between devices  6.76 us (6%)
  matrix products  4.5 us (4%)
  other arithmetic  2.03 us (2%)
    all_to_all x3, blocking collectives, sent_and_summed(): lax.all_to_all(blocks, axis, split_axis=0, concat_axis=0, tiled=True)  37.9 us
    all_to_all x2, blocking collectives, gathered_rows(): lax.all_to_all(jnp.stack([columns] * lax.axis_size('tp')), 'tp', 0, 0)  27.9 us
    all_to_all x2, blocking collectives, copy_for_each(): lax.all_to_all(jnp.broadcast_to(value[None], (devices, *value.shape)), ax...  19.6 us
    all_to_all x1, waiting for transfers between devices, sent_and_summed(): lax.all_to_all(blocks, axis, split_axis=0, concat_axis=0, tiled=True)  7.3 us
    all_to_all x1, starting transfers between devices, sent_and_summed(): lax.all_to_all(blocks, axis, split_axis=0, concat_axis=0, tiled=True)  6.76 us
    unnamed x28, local copies, waits for them, and re-layouts  2.66 us
  transfers between devices with their start and end apart: 1, of which 1 were waited for; matrix products, arithmetic and copies ran while one was open for 0% of the time, Pallas kernels for 0%

profile of v1, /device:TPU:1, one launch (start us, length us, event | category | flops | bytes accessed | tf_op | source)
XLA Modules:
  0.0 113.7 jit_solution(1028293842848873642)
XLA Ops:
  0.6 0.7 stack.4
  1.4 17.5 %all_to_all.40 = bf16[16,128,16]{1,2,0:T(8,128)(2,1)S(1)} all-to-all(bf16[16,128,16]{1,2,0:T(8,128)(2,1)S(1)} %stack.4), channel_id=1, replica_groups=mesh['kv'=16,'tp'=16] {'tp'}, dimensions={0} | all-to-all | bytes 131072 | tf_op jit(solution)/shard_map/all_to_all | solution.py:68
  19.0 0.2 convert_element_type.183
  19.2 0.5 copy.39
  19.8 0.4 reshape.300
  20.2 0.2 copy-done.12
  20.6 0.8 fusion.3
  21.4 0.8 fusion.2
  22.1 0.8 fusion.1
  22.9 0.8 fusion
  23.7 0.6 constant_dynamic-update-slice_fusion
  24.4 6.8 %all-to-all-start.1 = ((bf16[16,8,769]{2,1,0:T(8,128)(2,1)}), bf16[16,8,769]{2,1,0:T(8,128)(2,1)S(1)}, u32[]{:S(2)}, u32[]{:S(2)}) async-start(bf16[16,8,769]{2,1,0:T(8,128)(2,1)} %constant_dynamic-update-slice_fusion), calls=%async_computation.1 | async-start | bytes 458752 | tf_op jit(solution)/shard_map/all_to_all | solution.py:19
  31.1 0.6 copy-done.13
  31.9 7.3 %all-to-all-done.1 = bf16[16,8,769]{2,1,0:T(8,128)(2,1)S(1)} async-done(((bf16[16,8,769]{2,1,0:T(8,128)(2,1)}), bf16[16,8,769]{2,1,0:T(8,128)(2,1)S(1)}, u32[]{:S(2)}, u32[]{:S(2)}) %all-to-all-start.1) | async-done | bytes 196896 | tf_op jit(solution)/shard_map/all_to_all | solution.py:19
  39.7 0.2 multiply_add_fusion
  39.9 0.5 fusion.4
  40.6 9.2 %all_to_all.41 = bf16[16,8,256]{2,1,0:T(8,128)(2,1)S(1)} all-to-all(bf16[16,8,256]{2,1,0:T(8,128)(2,1)S(1)} %broadcast_in_dim.4), channel_id=1, replica_groups=mesh['kv'=16,'tp'=16] {'kv'}, dimensions={0} | all-to-all | bytes 131072 | tf_op jit(solution)/shard_map/all_to_all | solution.py:36
  50.1 12.9 %all_to_all.42 = bf16[16,128,16]{1,2,0:T(8,128)(2,1)S(1)} all-to-all(bf16[16,128,16]{1,2,0:T(8,128)(2,1)S(1)} %bitcast.66), channel_id=1, replica_groups=mesh['kv'=16,'tp'=16] {'tp'}, dimensions={0} | all-to-all | bytes 131072 | tf_op jit(solution)/shard_map/all_to_all | solution.py:19
  63.0 0.7 copy-done.10
  63.7 10.4 %all_to_all.43 = bf16[16,128,16]{1,2,0:T(8,128)(2,1)S(1)} all-to-all(bf16[16,128,16]{1,2,0:T(8,128)(2,1)S(1)} %stack.5), channel_id=1, replica_groups=mesh['kv'=16,'tp'=16] {'tp'}, dimensions={0} | all-to-all | bytes 131072 | tf_op jit(solution)/shard_map/all_to_all | solution.py:68
  74.1 0.2 convert_element_type.184
  74.4 0.5 copy.42
  74.9 0.4 reshape.303
  75.3 0.2 copy-done.11
  75.5 0.3 convolution_convert_fusion
  75.8 0.7 copy-done.4
  76.5 0.3 convolution_convert_fusion.1
  77.0 12.3 %all_to_all.44 = bf16[16,8,1409]{2,1,0:T(8,128)(2,1)S(1)} all-to-all(bf16[16,8,1409]{2,1,0:T(8,128)(2,1)S(1)} %concatenate.47), channel_id=1, replica_groups=mesh['kv'=16,'tp'=16] {'kv'}, dimensions={0} | all-to-all | bytes 721408 | tf_op jit(solution)/shard_map/all_to_all | solution.py:19
  89.6 10.4 %all_to_all.45 = bf16[16,8,704]{2,1,0:T(8,128)(2,1)S(1)} all-to-all(bf16[16,8,704]{2,1,0:T(8,128)(2,1)S(1)} %broadcast_in_dim.5), channel_id=1, replica_groups=mesh['kv'=16,'tp'=16] {'kv'}, dimensions={0} | all-to-all | bytes 360448 | tf_op jit(solution)/shard_map/all_to_all | solution.py:36
  100.0 0.2 convolution_convert_fusion.2
  100.4 12.7 %all_to_all.46 = bf16[16,128,16]{1,2,0:T(8,128)(2,1)S(1)} all-to-all(bf16[16,128,16]{1,2,0:T(8,128)(2,1)S(1)} %bitcast.67), channel_id=1, replica_groups=mesh['kv'=16,'tp'=16] {'tp'}, dimensions={0} | all-to-all | bytes 131072 | tf_op jit(solution)/shard_map/all_to_all | solution.py:19
  113.1 0.6 add_convert_fusion
  (55 shorter events, 2.1 us)
Async XLA Ops:
  0.6 74.7 %copy-start = (bf16[256,704]{0,1:T(8,128)(2,1)S(1)}, bf16[256,704]{0,1:T(8,128)(2,1)}, u32[]{:S(2)}) copy-start(bf16[256,704]{0,1:T(8,128)(2,1)} %param.24) | copy-start | bytes 1081348
  19.7 0.7 copy-start.12
  19.7 0.8 copy-start.8
  19.8 1.6 %copy-start.9 = (bf16[256,128]{1,0:T(8,128)(2,1)S(1)}, bf16[256,128]{1,0:T(8,128)(2,1)}, u32[]{:S(2)}) copy-start(bf16[256,128]{1,0:T(8,128)(2,1)} %param.18) | copy-start | bytes 196612
  19.8 2.4 %copy-start.5 = (bf16[256,256]{1,0:T(8,128)(2,1)S(1)}, bf16[256,256]{1,0:T(8,128)(2,1)}, u32[]{:S(2)}) copy-start(bf16[256,256]{1,0:T(8,128)(2,1)} %param.19) | copy-start | bytes 393220
  19.8 3.2 %copy-start.6 = (bf16[256,256]{1,0:T(8,128)(2,1)S(1)}, bf16[256,256]{1,0:T(8,128)(2,1)}, u32[]{:S(2)}) copy-start(bf16[256,256]{1,0:T(8,128)(2,1)} %param.20) | copy-start | bytes 393220
  20.4 19.3 %copy-start.2 = (f32[8,1,128,256]{3,2,1,0:T(8,128)S(1)}, f32[8,1,128,256]{3,2,1,0:T(8,128)}, u32[]{:S(2)}) copy-start(f32[8,1,128,256]{3,2,1,0:T(8,128)} %param.15) | copy-start | bytes 3145732
  24.4 14.8 %all-to-all-start.1 = ((bf16[16,8,769]{2,1,0:T(8,128)(2,1)}), bf16[16,8,769]{2,1,0:T(8,128)(2,1)S(1)}, u32[]{:S(2)}, u32[]{:S(2)}) async-start(bf16[16,8,769]{2,1,0:T(8,128)(2,1)} %constant_dynamic-update-slice_fusion), calls=%async_computation.1 | async-start | bytes 458752 | tf_op jit(solution)/shard_map/all_to_all | solution.py:19
  31.1 0.7 copy-start.13
  39.9 34.2 %copy-start.1 = (f32[8,1,128,256]{3,2,1,0:T(8,128)}, f32[8,1,128,256]{3,2,1,0:T(8,128)S(1)}, u32[]{:S(2)}) copy-start(f32[8,1,128,256]{3,2,1,0:T(8,128)S(1)} %multiply_add_fusion) | copy-start | bytes 3145732
  40.4 9.4 %copy-start.7 = (bf16[256,256]{1,0:T(8,128)(2,1)S(1)}, bf16[256,256]{1,0:T(8,128)(2,1)}, u32[]{:S(2)}) copy-start(bf16[256,256]{1,0:T(8,128)(2,1)} %param.21) | copy-start | bytes 393220
  63.0 0.7 copy-start.10
  74.9 0.7 copy-start.11
  75.5 1.0 copy-start.4
  89.5 10.6 %copy-start.3 = (bf16[704,256]{1,0:T(8,128)(2,1)S(1)}, bf16[704,256]{1,0:T(8,128)(2,1)}, u32[]{:S(2)}) copy-start(bf16[704,256]{1,0:T(8,128)(2,1)} %param.25) | copy-start | bytes 1081348
